TPU v7x, 32 devices: a whole 2x2x4 slice. The times are simulated.
32 devices in a mesh: grp: 2 (over y), fs: 4 (over z), tp: 4 (over x, core).
Axes of the slice: x: 2, y: 2, z: 4, core: 2. Of those that a mesh axis runs over, the one named last changes fastest.
Arguments:
- layer_input: bfloat16 [3072, 2048], P(('grp', 'fs'), 'tp'), parts along dimension 0, may hold values from -6 to 6
- first_gain: bfloat16 [1, 2048], P(None, 'tp'), may hold values from 0.099609375 to 1.8984375
- ffn_gate_w: bfloat16 [2048, 6144], P('fs', 'tp'), may hold values from -0.125 to 0.125
- ffn_up_w: bfloat16 [2048, 6144], P('fs', 'tp'), may hold values from -0.125 to 0.125
- ffn_down_w: bfloat16 [6144, 2048], P('tp', 'fs'), may hold values from -0.078125 to 0.078125
- mixer_gain: bfloat16 [1, 2048], P(None, 'tp'), may hold values from 0.099609375 to 1.8984375
- pool_in_w: bfloat16 [2048, 1024], P('fs', 'tp'), may hold values from -0.125 to 0.125
- mixer_gate_w: bfloat16 [2048, 2048], P('fs', 'tp'), may hold values from -0.125 to 0.125
- group_mix_w: bfloat16 [8, 128, 128], P('tp'), may hold values from -0.5 to 0.5
- pool_scale: float32 [1, 1024], P(None, 'tp'), may hold values from 0.1 to 1.9
- mixer_out_w: bfloat16 [1024, 2048], P('tp', 'fs'), may hold values from -0.1875 to 0.1875
- second_gain: bfloat16 [1, 2048], P(None, 'tp'), may hold values from 0.099609375 to 1.8984375
Outputs:
- layer_output: bfloat16 [3072, 2048], P(('grp', 'fs'), 'tp'), parts along dimension 0
There are 2 independent parts, one for each index of `grp`. A program takes and returns all parts, laid end to end along the dimension named above; an argument that names none is the same for every part. Nothing has to cross between parts.
All inputs are finite; a program needn't handle non-finite values.
Results may differ from a plain program's by a relative error of at most 0.015.
Values may be sent and summed in bfloat16 or wider, within the bound.
A program may use at most 64 MiB of HBM per device.

v0:
```python
import jax
import jax.numpy as jnp
from jax import lax
from jax.sharding import PartitionSpec as P


def norm_rows(values, gain):
    gathered, gain_whole = (
        lax.all_gather(values, "tp", axis=1, tiled=True),
        lax.all_gather(gain, "tp", axis=1, tiled=True),
    )
    widened = gathered.astype(jnp.float32)
    scaled = (widened * gain_whole.astype(jnp.float32)).astype(jnp.bfloat16)
    factor = lax.rsqrt(jnp.mean(widened * widened, axis=1, keepdims=True) + 1e-06)
    return (scaled, factor)


def column_sums(partial_value):
    return lax.psum_scatter(
        partial_value.astype(jnp.bfloat16), "tp", scatter_dimension=1, tiled=True
    ).astype(jnp.float32)


def add_pair(scaled, pieces):
    first_sum = jnp.dot(scaled, pieces[0], preferred_element_type=jnp.float32)
    second_sum = jnp.dot(scaled, pieces[1], preferred_element_type=jnp.float32)
    return (first_sum, second_sum)


def per_device(
    layer_input,
    first_gain,
    ffn_gate_w,
    ffn_up_w,
    ffn_down_w,
    mixer_gain,
    pool_in_w,
    mixer_gate_w,
    group_mix_w,
    pool_scale,
    mixer_out_w,
    second_gain,
):
    row_count = layer_input.shape[0]

    def feed_forward(values, gain):
        scaled, factor = norm_rows(values, gain)
        gate_sum, up_sum = add_pair(
            scaled,
            (
                lax.all_gather(ffn_gate_w, "fs", axis=0, tiled=True),
                lax.all_gather(ffn_up_w, "fs", axis=0, tiled=True),
            ),
        )
        hidden = (jax.nn.silu(factor * gate_sum) * (factor * up_sum)).astype(jnp.bfloat16)
        return jnp.dot(
            hidden,
            lax.all_gather(ffn_down_w, "fs", axis=1, tiled=True),
            preferred_element_type=jnp.float32,
        )

    first = (
        layer_input.astype(jnp.float32) + 0.5 * column_sums(feed_forward(layer_input, first_gain))
    ).astype(jnp.bfloat16)
    scaled, factor = norm_rows(first, mixer_gain)
    pool_sum, gate_sum = add_pair(
        scaled,
        (
            lax.all_gather(pool_in_w, "fs", axis=0, tiled=True),
            lax.all_gather(mixer_gate_w, "fs", axis=0, tiled=True),
        ),
    )
    pool_pre = (factor * pool_sum).astype(jnp.bfloat16)
    gate_logit = factor * gate_sum
    group_count = group_mix_w.shape[0]
    group_width = group_mix_w.shape[1]
    first_group = lax.axis_index("tp") * group_count
    values = pool_pre.astype(jnp.float32).reshape(row_count, group_count, group_width)
    running = jnp.cumsum(values, axis=0)
    positions = jnp.arange(row_count, dtype=jnp.int32)
    windows = 2 ** (1 + (first_group + jnp.arange(group_count, dtype=jnp.int32)) % 4)
    chosen = jnp.zeros_like(values)
    for span in (2, 4, 8, 16):
        lagged = jnp.pad(running, ((span, 0), (0, 0), (0, 0)))[:row_count]
        counts = jnp.minimum(positions + 1, span).astype(jnp.float32)[:, None, None]
        means = (running - lagged) / counts
        chosen = jnp.where((windows == span)[None, :, None], means, chosen)
    trail = (chosen - values).astype(jnp.bfloat16)
    mixed = jnp.einsum("tgc,gcd->tgd", trail, group_mix_w, preferred_element_type=jnp.float32)
    pooled = (mixed.reshape(row_count, group_count * group_width) * pool_scale).astype(jnp.bfloat16)
    lifted = column_sums(
        jnp.dot(
            pooled,
            lax.all_gather(mixer_out_w, "fs", axis=1, tiled=True),
            preferred_element_type=jnp.float32,
        )
    )
    second = (first.astype(jnp.float32) + jax.nn.sigmoid(gate_logit) * lifted).astype(jnp.bfloat16)
    result = second.astype(jnp.float32) + 0.5 * column_sums(feed_forward(second, second_gain))
    return result.astype(jnp.bfloat16)


def solution(mesh):
    return jax.shard_map(
        per_device,
        mesh=mesh,
        in_specs=(
            P(("grp", "fs"), "tp"),
            P(None, "tp"),
            P("fs", "tp"),
            P("fs", "tp"),
            P("tp", "fs"),
            P(None, "tp"),
            P("fs", "tp"),
            P("fs", "tp"),
            P("tp", None, None),
            P(None, "tp"),
            P("tp", "fs"),
            P(None, "tp"),
        ),
        out_specs=P(("grp", "fs"), "tp"),
        check_vma=False,
    )
```

profile of v0, /device:TPU:0, one launch (start us, length us, event | category | flops | bytes accessed | tf_op | source)
XLA Modules:
  0.0 653.4 jit_solution(9304917217902213386)
XLA Ops:
  9.4 6.2 all_gather.40
  15.6 15.7 %all-gather.10.cloned.1.call-done = bf16[384,2048]{1,0:T(8,128)(2,1)} async-done(((bf16[384,512]{1,0:T(8,128)(2,1)}), bf16[384,2048]{1,0:T(8,128)(2,1)}) %all-gather.10.cloned.1.call-update) | async-done | bytes 1572880 | tf_op jit(solution)/shard_map/all_gather | solution.py:9
  33.1 115.1 %all-gather.12.cloned.1.call-done = bf16[2048,1536]{1,0:T(8,128)(2,1)} async-done(((bf16[512,1536]{1,0:T(8,128)(2,1)}), bf16[2048,1536]{1,0:T(8,128)(2,1)}) %all-gather.12.cloned.1.call-update) | async-done | bytes 6291472 | tf_op jit(solution)/shard_map/all_gather | solution.py:51
  148.2 7.4 %convolution_multiply_fusion.3 = f32[384,1536]{1,0:T(8,128)} fusion(bf16[2048,1536]{1,0:T(8,128)(2,1)} %all-gather.12.cloned.1.call-done, bf16[384,2048]{1,0:T(8,128)(2,1)} %all-gather.10.cloned.1.call-done, f32[2048]{0:T(1024)S(1)} %bitcast.38, f32[384]{0:T(512)S(1)} %add_rsqrt_fusion.2), kind=kOutput, calls=%fused_computation.17 | convolution fusion | flops 2418868224 | bytes 10233344 | tf_op jit(solution)/shard_map/dot_general | solution.py:25
  155.6 107.7 %all-gather.14.cloned.1.call-done = bf16[2048,1536]{1,0:T(8,128)(2,1)} async-done(((bf16[512,1536]{1,0:T(8,128)(2,1)}), bf16[2048,1536]{1,0:T(8,128)(2,1)}) %all-gather.14.cloned.1.call-update) | async-done | bytes 6291472 | tf_op jit(solution)/shard_map/all_gather | solution.py:52
  263.3 115.0 %all-gather.16.cloned.1.call-done = bf16[1536,2048]{1,0:T(8,128)(2,1)} async-done(((bf16[1536,512]{1,0:T(8,128)(2,1)}), bf16[1536,2048]{1,0:T(8,128)(2,1)}) %all-gather.16.cloned.1.call-update) | async-done | bytes 6291472 | tf_op jit(solution)/shard_map/all_gather | solution.py:58
  378.3 11.6 %convolution_convert_fusion.2 = bf16[384,2048]{1,0:T(8,128)(2,1)} fusion(bf16[1536,2048]{1,0:T(8,128)(2,1)} %all-gather.16.cloned.1.call-done, bf16[2048,1536]{1,0:T(8,128)(2,1)} %all-gather.14.cloned.1.call-done, f32[384,1536]{1,0:T(8,128)} %convolution_multiply_fusion.3, bf16[384,2048]{1,0:T(8,128)(2,1)S(1)} %copy-done.2, f32[2048]{0:T(1024)S(1)} %bitcast.39, ...), kind=kOutput, calls=%fused_computation.22 | convolution fusion | flops 4839112704 | bytes 18097664 | tf_op jit(solution)/shard_map/dot_general | solution.py:56
  390.0 26.3 %reduce-scatter.4.cloned.1.call-done = bf16[384,512]{1,0:T(8,128)(2,1)} async-done(((bf16[384,2048]{1,0:T(8,128)(2,1)}), bf16[384,512]{1,0:T(8,128)(2,1)}) %reduce-scatter.4.cloned.1.call-update) | async-done | bytes 393232 | tf_op jit(solution)/shard_map/reduce_scatter | solution.py:19
  416.3 1.9 add_convert_fusion.1
  420.5 5.2 all_gather.45
  425.7 12.2 %all-gather.18.cloned.1.call-done = bf16[384,2048]{1,0:T(8,128)(2,1)} async-done(((bf16[384,512]{1,0:T(8,128)(2,1)}), bf16[384,2048]{1,0:T(8,128)(2,1)}) %all-gather.18.cloned.1.call-update) | async-done | bytes 1572880 | tf_op jit(solution)/shard_map/all_gather | solution.py:9
  439.7 27.8 %all-gather.22.cloned.1.call-done = bf16[2048,256]{1,0:T(8,128)(2,1)} async-done(((bf16[512,256]{1,0:T(8,128)(2,1)}), bf16[2048,256]{1,0:T(8,128)(2,1)}) %all-gather.22.cloned.1.call-update) | async-done | bytes 1048592 | tf_op jit(solution)/shard_map/all_gather | solution.py:69
  467.5 2.5 fusion.45
  471.5 25.0 %all-gather.24.cloned.1.call-done = bf16[256,2048]{1,0:T(8,128)(2,1)} async-done(((bf16[256,512]{1,0:T(8,128)(2,1)}), bf16[256,2048]{1,0:T(8,128)(2,1)}) %all-gather.24.cloned.1.call-update) | async-done | bytes 1048592 | tf_op jit(solution)/shard_map/all_gather | solution.py:94
  496.5 3.0 convolution_convert_fusion.1
  499.5 43.6 %all-gather.20.cloned.1.call-done = bf16[2048,512]{1,0:T(8,128)(2,1)} async-done(((bf16[512,512]{1,0:T(8,128)(2,1)}), bf16[2048,512]{1,0:T(8,128)(2,1)}) %all-gather.20.cloned.1.call-update) | async-done | bytes 2097168 | tf_op jit(solution)/shard_map/all_gather | solution.py:70
  543.1 29.2 %reduce-scatter.6.cloned.1.call-done = bf16[384,512]{1,0:T(8,128)(2,1)} async-done(((bf16[384,2048]{1,0:T(8,128)(2,1)}), bf16[384,512]{1,0:T(8,128)(2,1)}) %reduce-scatter.6.cloned.1.call-update) | async-done | bytes 393232 | tf_op jit(solution)/shard_map/reduce_scatter | solution.py:19
  572.4 3.5 fusion.42
  576.0 5.4 all_gather.50
  581.4 14.3 %all-gather.26.cloned.1.call-done = bf16[384,2048]{1,0:T(8,128)(2,1)} async-done(((bf16[384,512]{1,0:T(8,128)(2,1)}), bf16[384,2048]{1,0:T(8,128)(2,1)}) %all-gather.26.cloned.1.call-update) | async-done | bytes 1572880 | tf_op jit(solution)/shard_map/all_gather | solution.py:9
  597.5 7.4 %convolution_multiply_fusion.1 = f32[384,1536]{1,0:T(8,128)} fusion(bf16[2048,1536]{1,0:T(8,128)(2,1)} %all-gather.12.cloned.1.call-done, bf16[384,2048]{1,0:T(8,128)(2,1)} %all-gather.26.cloned.1.call-done, f32[2048]{0:T(1024)S(1)} %bitcast.40, f32[384]{0:T(512)S(1)} %add_rsqrt_fusion), kind=kOutput, calls=%fused_computation.14 | convolution fusion | flops 2418868224 | bytes 10233344 | tf_op jit(solution)/shard_map/dot_general | solution.py:25
  604.9 11.6 %convolution_convert_fusion = bf16[384,2048]{1,0:T(8,128)(2,1)} fusion(bf16[1536,2048]{1,0:T(8,128)(2,1)} %all-gather.16.cloned.1.call-done, bf16[2048,1536]{1,0:T(8,128)(2,1)} %all-gather.14.cloned.1.call-done, f32[384,1536]{1,0:T(8,128)} %convolution_multiply_fusion.1, bf16[384,2048]{1,0:T(8,128)(2,1)S(1)} %copy-done.3, f32[2048]{0:T(1024)S(1)} %bitcast.41, ...), kind=kOutput, calls=%fused_computation.20 | convolution fusion | flops 4839112704 | bytes 18097664 | tf_op jit(solution)/shard_map/dot_general | solution.py:56
  616.6 28.1 %reduce-scatter.8.cloned.1.call-done = bf16[384,512]{1,0:T(8,128)(2,1)} async-done(((bf16[384,2048]{1,0:T(8,128)(2,1)}), bf16[384,512]{1,0:T(8,128)(2,1)}) %reduce-scatter.8.cloned.1.call-update) | async-done | bytes 393232 | tf_op jit(solution)/shard_map/reduce_scatter | solution.py:19
  644.7 1.9 add_convert_fusion
  (67 shorter events, 12.1 us)
Async XLA Ops:
  6.5 464.1 %copy-start = (bf16[2,128,128]{2,1,0:T(8,128)(2,1)S(1)}, bf16[2,128,128]{2,1,0:T(8,128)(2,1)}, u32[]{:S(2)}) copy-start(bf16[2,128,128]{2,1,0:T(8,128)(2,1)} %param.20) | copy-start | bytes 196612
  6.5 24.7 %all-gather.10.cloned.1.call-start = ((), (), s32[]{:S(2)}) async-start(), calls=%async_computation.3 | async-start | bytes 1966080 | tf_op jit(solution)/shard_map/all_gather | solution.py:9
  7.3 2.1 copy-start.7
  7.3 140.9 %all-gather.12.cloned.1.call-start = ((), (), s32[]{:S(2)}) async-start(), calls=%async_computation.4 | async-start | bytes 7864320 | tf_op jit(solution)/shard_map/all_gather | solution.py:51
  8.0 255.3 %all-gather.14.cloned.1.call-start = ((), (), s32[]{:S(2)}) async-start(), calls=%async_computation.5 | async-start | bytes 7864320 | tf_op jit(solution)/shard_map/all_gather | solution.py:52
  8.8 369.6 %all-gather.16.cloned.1.call-start = ((), (), s32[]{:S(2)}) async-start(), calls=%async_computation.6 | async-start | bytes 7864320 | tf_op jit(solution)/shard_map/all_gather | solution.py:58
  9.3 406.9 %reduce-scatter.4.cloned.1.call-start = ((), (), s32[]{:S(2)}) async-start(), calls=%async_computation.7 | async-start | bytes 1966080 | tf_op jit(solution)/shard_map/reduce_scatter | solution.py:19
  148.2 230.1 %copy-start.2 = (bf16[384,2048]{1,0:T(8,128)(2,1)S(1)}, bf16[384,2048]{1,0:T(8,128)(2,1)}, u32[]{:S(2)}) copy-start(bf16[384,2048]{1,0:T(8,128)(2,1)} %all-gather.10.cloned.1.call-done) | copy-start | bytes 4718596
  155.6 260.7 %copy-start.4 = (bf16[384,512]{1,0:T(8,128)(2,1)S(1)}, bf16[384,512]{1,0:T(8,128)(2,1)}, u32[]{:S(2)}) copy-start(bf16[384,512]{1,0:T(8,128)(2,1)} %param.12) | copy-start | bytes 1179652
  389.9 30.5 %copy-start.8 = (bf16[1,512]{1,0:T(2,128)(2,1)S(1)}, bf16[1,512]{1,0:T(2,128)(2,1)}, u32[]{:S(2)}) copy-start(bf16[1,512]{1,0:T(2,128)(2,1)} %param.17) | copy-start | bytes 3076
  389.9 48.0 %all-gather.18.cloned.1.call-start = ((), (), s32[]{:S(2)}) async-start(), calls=%async_computation.8 | async-start | bytes 1966080 | tf_op jit(solution)/shard_map/all_gather | solution.py:9
  418.2 49.4 %all-gather.22.cloned.1.call-start = ((), (), s32[]{:S(2)}) async-start(), calls=%async_computation.10 | async-start | bytes 1310720 | tf_op jit(solution)/shard_map/all_gather | solution.py:69
  418.9 77.6 %all-gather.24.cloned.1.call-start = ((), (), s32[]{:S(2)}) async-start(), calls=%async_computation.11 | async-start | bytes 1310720 | tf_op jit(solution)/shard_map/all_gather | solution.py:94
  419.7 123.5 %all-gather.20.cloned.1.call-start = ((), (), s32[]{:S(2)}) async-start(), calls=%async_computation.9 | async-start | bytes 2621440 | tf_op jit(solution)/shard_map/all_gather | solution.py:70
  420.4 152.0 %reduce-scatter.6.cloned.1.call-start = ((), (), s32[]{:S(2)}) async-start(), calls=%async_computation.12 | async-start | bytes 1966080 | tf_op jit(solution)/shard_map/reduce_scatter | solution.py:19
  470.7 0.7 copy-start.10
  471.3 101.0 %copy-start.1 = (bf16[384,2048]{1,0:T(8,128)(2,1)S(1)}, bf16[384,2048]{1,0:T(8,128)(2,1)}, u32[]{:S(2)}) copy-start(bf16[384,2048]{1,0:T(8,128)(2,1)} %all-gather.18.cloned.1.call-done) | copy-start | bytes 4718596
  471.3 101.0 %copy-start.5 = (bf16[384,512]{1,0:T(8,128)(2,1)S(1)}, bf16[384,512]{1,0:T(8,128)(2,1)}, u32[]{:S(2)}) copy-start(bf16[384,512]{1,0:T(8,128)(2,1)} %add_convert_fusion.1) | copy-start | bytes 1179652
  499.5 76.5 %copy-start.9 = (bf16[1,512]{1,0:T(2,128)(2,1)S(1)}, bf16[1,512]{1,0:T(2,128)(2,1)}, u32[]{:S(2)}) copy-start(bf16[1,512]{1,0:T(2,128)(2,1)} %param.23) | copy-start | bytes 3076
  499.5 96.2 %all-gather.26.cloned.1.call-start = ((), (), s32[]{:S(2)}) async-start(), calls=%async_computation.13 | async-start | bytes 1966080 | tf_op jit(solution)/shard_map/all_gather | solution.py:9
  575.9 68.8 %reduce-scatter.8.cloned.1.call-start = ((), (), s32[]{:S(2)}) async-start(), calls=%async_computation.14 | async-start | bytes 1966080 | tf_op jit(solution)/shard_map/reduce_scatter | solution.py:19
  597.5 7.4 %copy-start.3 = (bf16[384,2048]{1,0:T(8,128)(2,1)S(1)}, bf16[384,2048]{1,0:T(8,128)(2,1)}, u32[]{:S(2)}) copy-start(bf16[384,2048]{1,0:T(8,128)(2,1)} %all-gather.26.cloned.1.call-done) | copy-start | bytes 4718596
  604.9 39.8 %copy-start.6 = (bf16[384,512]{1,0:T(8,128)(2,1)S(1)}, bf16[384,512]{1,0:T(8,128)(2,1)}, u32[]{:S(2)}) copy-start(bf16[384,512]{1,0:T(8,128)(2,1)} %fusion.42) | copy-start | bytes 1179652
Sparse Core Ops, SparseCore 0:
  8.9 22.3 all-gather.9
  32.9 115.3 all-gather.11
  149.8 113.5 all-gather.13
  264.8 113.4 all-gather.15
  390.1 26.1 reduce-scatter.3
  418.3 19.6 all-gather.17
  439.5 27.9 all-gather.21
  469.1 27.3 all-gather.23
  498.1 45.0 all-gather.19
  545.5 26.8 reduce-scatter.5
  576.0 19.6 all-gather.25
  616.7 27.9 reduce-scatter.7
where the time goes:
time: 654 us; the launch traced here: 653 us
  waiting for transfers between devices  565 us (86%)
  matrix products  47.6 us (7%)
  blocking collectives  16.7 us (3%)
  between operations  13.7 us (2%)
  other arithmetic  9.71 us (1%)
    all_gather x1, waiting for transfers between devices, feed_forward(): lax.all_gather(ffn_gate_w, 'fs', axis=0, tiled=True)  115 us
    all_gather x1, waiting for transfers between devices, feed_forward(): lax.all_gather(ffn_down_w, 'fs', axis=1, tiled=True)  115 us
    all_gather x1, waiting for transfers between devices, feed_forward(): lax.all_gather(ffn_up_w, 'fs', axis=0, tiled=True)  108 us
    reduce_scatter x3, waiting for transfers between devices, column_sums(): lax.psum_scatter(partial_value.astype(jnp.bfloat16), 'tp', scatter_dimens...  83.7 us
    all_gather x1, waiting for transfers between devices, per_device(): lax.all_gather(mixer_gate_w, 'fs', axis=0, tiled=True)  43.6 us
    all_gather x3, waiting for transfers between devices, norm_rows(): lax.all_gather(values, 'tp', axis=1, tiled=True)  42.2 us
    all_gather x1, waiting for transfers between devices, per_device(): lax.all_gather(pool_in_w, 'fs', axis=0, tiled=True)  27.8 us
    all_gather x1, waiting for transfers between devices, per_device(): lax.all_gather(mixer_out_w, 'fs', axis=1, tiled=True)  25 us
  transfers between devices with their start and end apart: 12, of which 12 were waited for; matrix products, arithmetic and copies ran while one was open for 3% of the time, Pallas kernels for 0%

commit v1 on v0

v1 whole, which is shorter than its diff:
```python
import functools

import jax
import jax.numpy as jnp
from jax import lax
from jax.experimental import pallas as pl
from jax.experimental.pallas import tpu as pltpu
from jax.sharding import PartitionSpec as P

MESH = pl.DeviceIdType.MESH
F32 = jnp.float32
BF16 = jnp.bfloat16
GAIN_ROWS = 16


def ceil_pieces(rows, wanted):
    while rows % (wanted * 16) != 0:
        wanted -= 1
    return wanted


def layer_kernel(
    sizes,
    payload,
    gate_w,
    up_w,
    down_w,
    pool_w,
    mgate_w,
    mout_w,
    mix_w,
    scale_w,
    out,
    gate_all,
    up_all,
    down_all,
    pool_all,
    mgate_all,
    mout_all,
    input_all,
    value_all,
    scaled,
    factor,
    hidden,
    pooled,
    logit,
    parts,
    sums,
    local_sem,
    z_recv,
    y_recv,
    up_sem,
    low_sem,
    y_sem,
    x_send,
    x_recv,
    s_send,
    s_recv,
):
    grps, planes, tps, piece_counts = sizes
    g = lax.axis_index("grp")
    f = lax.axis_index("fs")
    tp = lax.axis_index("tp")
    rows, width = out.shape
    chips = tps // 2
    chip, core = tp // 2, tp % 2
    peers = [
        ((chip + i) % chips) * 2 + (core + b) % 2 for i in range(1, chips) for b in range(2)
    ] + [chip * 2 + (core + 1) % 2]
    other_grps = [(g + d) % grps for d in range(1, grps)]

    barrier = pltpu.get_barrier_semaphore()
    for peer in peers:
        pl.semaphore_signal(barrier, inc=1, device_id={"tp": peer}, device_id_type=MESH)
    for other in other_grps:
        pl.semaphore_signal(barrier, inc=1, device_id={"grp": other}, device_id_type=MESH)

    @pl.when(f > 0)
    def _():
        pl.semaphore_signal(barrier, inc=1, device_id={"fs": f - 1}, device_id_type=MESH)

    @pl.when(f < planes - 1)
    def _():
        pl.semaphore_signal(barrier, inc=1, device_id={"fs": f + 1}, device_id_type=MESH)

    inner = jnp.where(f > 0, 1, 0) + jnp.where(f < planes - 1, 1, 0)
    pl.semaphore_wait(barrier, len(peers) + len(other_grps) + inner)

    def value_copy(phase, peer, slot):
        ref = input_all if phase == 0 else value_all.at[phase - 1]
        return pltpu.make_async_remote_copy(
            src_ref=payload if phase == 0 else ref.at[tp],
            dst_ref=ref.at[slot],
            send_sem=x_send.at[phase, peer],
            recv_sem=x_recv.at[phase, slot],
            device_id={"tp": peer},
            device_id_type=MESH,
        )

    def sum_copy(phase, peer, slot):
        return pltpu.make_async_remote_copy(
            src_ref=parts.at[phase, peer],
            dst_ref=sums.at[phase, slot],
            send_sem=s_send.at[phase, peer],
            recv_sem=s_recv.at[phase, slot],
            device_id={"tp": peer},
            device_id_type=MESH,
        )

    weights = (
        (gate_w, gate_all, False),
        (up_w, up_all, False),
        (down_w, down_all, True),
        (pool_w, pool_all, False),
        (mgate_w, mgate_all, False),
        (mout_w, mout_all, True),
    )
    pieces = []
    for number, (shard, whole, stacked) in enumerate(weights):
        for part in range(piece_counts[number]):
            pieces.append((number, part))

    def place(piece, plane, grp):
        number, part = pieces[piece]
        shard, whole, stacked = weights[number]
        tall = shard.shape[0]
        half = tall // grps
        size = half // piece_counts[number]
        start = grp * half + part * size
        if stacked:
            return whole.at[plane, pl.ds(pl.multiple_of(start, 16), size), :]
        return whole.at[pl.ds(pl.multiple_of(plane * tall + start, 16), size), :]

    def own_place(piece):
        number, part = pieces[piece]
        shard = weights[number][0]
        half = shard.shape[0] // grps
        size = half // piece_counts[number]
        return shard.at[pl.ds(pl.multiple_of(g * half + part * size, 16), size), :]

    def z_copy(piece, plane, step, own=False):
        spot = place(piece, plane, g)
        return pltpu.make_async_remote_copy(
            src_ref=own_place(piece) if own else spot,
            dst_ref=spot,
            send_sem=(up_sem if step > 0 else low_sem).at[piece, plane],
            recv_sem=z_recv.at[piece, plane],
            device_id={"fs": f + step},
            device_id_type=MESH,
        )

    def y_copy(piece, plane, number, source):
        spot = place(piece, plane, source)
        return pltpu.make_async_remote_copy(
            src_ref=spot,
            dst_ref=spot,
            send_sem=y_sem.at[piece, plane, number],
            recv_sem=y_recv.at[piece, plane, source],
            device_id={"grp": other_grps[number]},
            device_id_type=MESH,
        )

    def send_own(piece):
        if piece >= len(pieces):
            return

        @pl.when(f < planes - 1)
        def _():
            z_copy(piece, f, 1, own=True).start()

        @pl.when(f > 0)
        def _():
            z_copy(piece, f, -1, own=True).start()

    def pass_on(piece):
        send_own(piece + 2)
        for hop in range(1, planes):

            @pl.when(f >= hop)
            def _():
                z_copy(piece, f - hop, -1).wait_recv()

                @pl.when(f < planes - 1)
                def _():
                    z_copy(piece, f - hop, 1).start()

                for number in range(len(other_grps)):
                    y_copy(piece, f - hop, number, g).start()

            @pl.when(f + hop < planes)
            def _():
                z_copy(piece, f + hop, 1).wait_recv()

                @pl.when(f > 0)
                def _():
                    z_copy(piece, f + hop, -1).start()

                for number in range(len(other_grps)):
                    y_copy(piece, f + hop, number, g).start()

    def of(*numbers):
        return [p for p, (number, part) in enumerate(pieces) if number in numbers]

    def arrive(*numbers):
        for number in numbers:
            shard, whole, stacked = weights[number]
            local_copy(number).wait()
        for piece in of(*numbers):
            for step in range(1, planes):
                plane = (f + step) % planes
                for number, other in enumerate(other_grps):
                    y_copy(piece, plane, number, other).wait_recv()

    def local_copy(number):
        shard, whole, stacked = weights[number]
        tall = shard.shape[0]
        spot = whole.at[f] if stacked else whole.at[pl.ds(pl.multiple_of(f * tall, 16), tall), :]
        return pltpu.make_async_copy(shard, spot, local_sem.at[number])

    def local_input():
        return pltpu.make_async_copy(payload, input_all.at[tp], local_sem.at[len(weights)])

    row_tile = 32

    def scale_values(phase):
        for peer in peers:
            value_copy(phase, peer, peer).wait_recv()
        ref = input_all if phase == 0 else value_all.at[phase - 1]

        def body(step, carry):
            span = pl.ds(pl.multiple_of(step * row_tile, row_tile), row_tile)
            total = jnp.zeros((row_tile, 1), F32)
            for t in range(tps):
                gains = input_all[t, rows : rows + GAIN_ROWS, :].astype(F32)
                value = ref[t, span, :].astype(F32)
                total = total + jnp.sum(value * value, axis=1, keepdims=True)
                scaled[span, t * width : (t + 1) * width] = (
                    value * gains[phase : phase + 1]
                ).astype(BF16)
            factor[span, :] = lax.rsqrt(total / (tps * width) + 1e-06)
            return carry

        lax.fori_loop(0, rows // row_tile, body, 0)

    def hidden_units():
        units = hidden.shape[1]
        tile = 256 if units % 256 == 0 else 128

        def body(step, carry):
            span = pl.ds(pl.multiple_of(step * tile, tile), tile)
            gate = factor[...] * jnp.dot(
                scaled[...], gate_all[:, span], preferred_element_type=F32
            )
            up = factor[...] * jnp.dot(scaled[...], up_all[:, span], preferred_element_type=F32)
            hidden[:, span] = (jax.nn.silu(gate) * up).astype(BF16)
            return carry

        lax.fori_loop(0, units // tile, body, 0)

    def project(phase, left, right_all):
        ratio = planes // tps
        block = right_all.shape[2]
        for peer in peers + [tp]:
            for piece in range(ratio):
                parts[phase, peer, :, piece * block : (piece + 1) * block] = jnp.dot(
                    left[...], right_all[peer * ratio + piece], preferred_element_type=F32
                ).astype(BF16)
            if peer is not tp:
                sum_copy(phase, peer, tp).start()

    def total_of(phase):
        for peer in peers:
            sum_copy(phase, peer, peer).wait_recv()
        total = parts[phase, tp].astype(F32)
        for peer in peers:
            total = total + sums[phase, peer].astype(F32)
        return total

    def spread(phase):
        for peer in peers:
            value_copy(phase, peer, tp).start()

    local_input().start()
    spread(0)
    send_own(0)
    send_own(1)
    for number in range(len(weights)):
        local_copy(number).start()
    first_pieces = of(0, 1)
    pass_on(first_pieces[0])
    local_input().wait()
    scale_values(0)
    for piece in first_pieces[1:]:
        pass_on(piece)
    for piece in of(2)[:1]:
        pass_on(piece)
    arrive(0, 1)
    hidden_units()
    for piece in of(2)[1:]:
        pass_on(piece)
    arrive(2)
    project(0, hidden, down_all)

    for piece in of(3):
        pass_on(piece)
    value_all[0, tp] = (
        input_all[tp, 0:rows, :].astype(F32) + 0.5 * total_of(0)
    ).astype(BF16)
    spread(1)
    for piece in of(4):
        pass_on(piece)
    scale_values(1)
    for piece in of(5):
        pass_on(piece)
    arrive(3, 4)
    groups, group_width = mix_w.shape[0], mix_w.shape[1]
    pool_pre = (
        factor[...] * jnp.dot(scaled[...], pool_all[...], preferred_element_type=F32)
    ).astype(BF16)
    position = lax.broadcasted_iota(jnp.int32, (rows, group_width), 0)
    for group in range(groups):
        span = slice(group * group_width, (group + 1) * group_width)
        value = pool_pre[:, span].astype(F32)
        kind = (tp * groups + group) % 4
        running = value
        chosen = jnp.zeros_like(value)
        for level in range(4):
            lag = 2**level
            running = running + jnp.where(
                position >= lag, pltpu.roll(running, lag, axis=0), 0.0
            )
            counts = jnp.minimum(position + 1, 2 * lag).astype(F32)
            chosen = jnp.where(kind == level, running / counts, chosen)
        trail = (chosen - value).astype(BF16)
        mixed = jnp.dot(trail, mix_w[group], preferred_element_type=F32)
        pooled[:, span] = (mixed * scale_w[:, span]).astype(BF16)
    arrive(5)
    project(1, pooled, mout_all)
    logit[...] = factor[...] * jnp.dot(scaled[...], mgate_all[...], preferred_element_type=F32)
    value_all[1, tp] = (
        value_all[0, tp].astype(F32) + jax.nn.sigmoid(logit[...]) * total_of(1)
    ).astype(BF16)

    spread(2)
    scale_values(2)
    hidden_units()
    project(2, hidden, down_all)
    out[...] = (value_all[1, tp].astype(F32) + 0.5 * total_of(2)).astype(BF16)

    for phase in range(3):
        for peer in peers:
            value_copy(phase, peer, tp).wait_send()
            sum_copy(phase, peer, tp).wait_send()
    for piece in range(len(pieces)):

        @pl.when(f < planes - 1)
        def _():
            z_copy(piece, f, 1, own=True).wait_send()

        @pl.when(f > 0)
        def _():
            z_copy(piece, f, -1, own=True).wait_send()

        for hop in range(1, planes):

            @pl.when(f >= hop)
            def _():
                @pl.when(f < planes - 1)
                def _():
                    z_copy(piece, f - hop, 1).wait_send()

                for number in range(len(other_grps)):
                    y_copy(piece, f - hop, number, g).wait_send()

            @pl.when(f + hop < planes)
            def _():
                @pl.when(f > 0)
                def _():
                    z_copy(piece, f + hop, -1).wait_send()

                for number in range(len(other_grps)):
                    y_copy(piece, f + hop, number, g).wait_send()


def per_device(
    grps,
    planes,
    tps,
    layer_input,
    first_gain,
    ffn_gate_w,
    ffn_up_w,
    ffn_down_w,
    mixer_gain,
    pool_in_w,
    mixer_gate_w,
    group_mix_w,
    pool_scale,
    mixer_out_w,
    second_gain,
):
    rows, width = layer_input.shape
    features = width * tps
    gains = jnp.concatenate([first_gain, mixer_gain, second_gain], axis=0)
    payload = jnp.concatenate(
        [layer_input, jnp.pad(gains, ((0, GAIN_ROWS - 3), (0, 0)))], axis=0
    )
    units = ffn_gate_w.shape[1]
    channels = pool_in_w.shape[1]
    wanted = (2, 2, 2, 1, 1, 1)
    shards = (ffn_gate_w, ffn_up_w, ffn_down_w, pool_in_w, mixer_gate_w, mixer_out_w)
    piece_counts = tuple(
        ceil_pieces(shard.shape[0] // grps, count) for shard, count in zip(shards, wanted)
    )
    n = sum(piece_counts)
    dma = pltpu.SemaphoreType.DMA
    whole = pl.BlockSpec(memory_space=pltpu.VMEM)
    remote = pl.BlockSpec(memory_space=pl.ANY)
    return pl.pallas_call(
        functools.partial(layer_kernel, (grps, planes, tps, piece_counts)),
        out_shape=jax.ShapeDtypeStruct((rows, width), BF16),
        in_specs=[remote] * 7 + [whole] * 2,
        out_specs=whole,
        scratch_shapes=[
            pltpu.VMEM((features, units), BF16),
            pltpu.VMEM((features, units), BF16),
            pltpu.VMEM((planes,) + ffn_down_w.shape, BF16),
            pltpu.VMEM((features, channels), BF16),
            pltpu.VMEM((features, width), BF16),
            pltpu.VMEM((planes,) + mixer_out_w.shape, BF16),
            pltpu.VMEM((tps, rows + GAIN_ROWS, width), BF16),
            pltpu.VMEM((2, tps, rows, width), BF16),
            pltpu.VMEM((rows, features), BF16),
            pltpu.VMEM((rows, 1), F32),
            pltpu.VMEM((rows, units), BF16),
            pltpu.VMEM((rows, channels), BF16),
            pltpu.VMEM((rows, width), F32),
            pltpu.VMEM((3, tps, rows, width), BF16),
            pltpu.VMEM((3, tps, rows, width), BF16),
            dma((len(shards) + 1,)),
            dma((n, planes)),
            dma((n, planes, grps)),
            dma((n, planes)),
            dma((n, planes)),
            dma((n, planes, max(grps - 1, 1))),
            dma((3, tps)),
            dma((3, tps)),
            dma((3, tps)),
            dma((3, tps)),
        ],
        compiler_params=pltpu.CompilerParams(
            collective_id=0, has_side_effects=True, vmem_limit_bytes=60 * 1024 * 1024
        ),
    )(payload, *shards, group_mix_w, pool_scale)


def solution(mesh):
    return jax.shard_map(
        functools.partial(
            per_device, mesh.shape["grp"], mesh.shape["fs"], mesh.shape["tp"]
        ),
        mesh=mesh,
        in_specs=(
            P(("grp", "fs"), "tp"),
            P(None, "tp"),
            P("fs", "tp"),
            P("fs", "tp"),
            P("tp", "fs"),
            P(None, "tp"),
            P("fs", "tp"),
            P("fs", "tp"),
            P("tp", None, None),
            P(None, "tp"),
            P("tp", "fs"),
            P(None, "tp"),
        ),
        out_specs=P(("grp", "fs"), "tp"),
        check_vma=False,
    )
```

time: 654 us -> 300 us (0.46)
  waiting for transfers between devices: 565 us -> 0 us
  Pallas kernels: 0 us -> 294 us
  matrix products: 47.6 us -> 0 us
  blocking collectives: 16.7 us -> 0 us
  between operations: 13.7 us -> 0.01 us
  other arithmetic: 9.71 us -> 2.49 us
    all_gather x9 -> x0, waiting for transfers between devices: 477 us -> none  [the longest x1 115 us: feed_forward(): lax.all_gather(ffn_gate_w, 'fs', axis=0, tiled=True)]
    pallas_call x0 -> x1, Pallas kernels: none -> 294 us  [per_device(): pl.pallas_call(functools.partial(layer_kernel, (grps, planes, tps, piece_...]
    reduce_scatter x3 -> x0, waiting for transfers between devices: 83.7 us -> none  [column_sums(): lax.psum_scatter(partial_value.astype(jnp.bfloat16), 'tp', scatter_dimens...]
    dot_general x8 -> x0, matrix products: 47.6 us -> none  [the longest x2 23.2 us: feed_forward(): jnp.dot(hidden, lax.all_gather(ffn_down_w, 'fs', axis=1, tiled=True), pre...]
    all_gather x3 -> x0, blocking collectives: 16.7 us -> none  [norm_rows(): lax.all_gather(gain, 'tp', axis=1, tiled=True)]
  transfers between devices with their start and end apart: 12 -> 0, of which waited for: 12 -> 0; matrix products, arithmetic and copies ran while one was open for 3% -> 0% of each run, Pallas kernels for 0% -> 0%
where the time goes in v1:
time: 300 us; the launch traced here: 298 us
  Pallas kernels  294 us (98%)
    pallas_call x1, Pallas kernels, per_device(): pl.pallas_call(functools.partial(layer_kernel, (grps, planes, tps, piece_...  294 us

profile of v1, /device:TPU:0, one launch (start us, length us, event | category | flops | bytes accessed | tf_op | source)
XLA Modules:
  0.0 298.0 jit_solution(6588346653265631842)
XLA Ops:
  0.0 0.7 fusion.4
  0.7 1.8 pad_maximum_fusion.payload
  2.5 293.8 %shard_map.118 = bf16[384,512]{1,0:T(8,128)(2,1)} custom-call(bf16[400,512]{1,0:T(8,128)(2,1)} %pad_maximum_fusion.payload, bf16[512,1536]{1,0:T(8,128)(2,1)} %gate_w.1, bf16[512,1536]{1,0:T(8,128)(2,1)} %up_w.1, bf16[1536,512]{1,0:T(8,128)(2,1)} %down_w.1, bf16[512,256]{1,0:T(8,128)(2,1)} %pool_w.1, bf16[512,512]{1,0:T(8,128)(2,1)} %mgate_w.1, ...), custom_call_target="tpu_custom_call" | custom-call | tf_op jit(solution)/shard_map/pallas_call | solution.py:419
  296.3 1.8 copy.14

commit v2 on v1

--- a/solution.py
+++ b/solution.py
@@ -53,6 +53,7 @@
     low_sem,
     y_sem,
     x_send,
+    x_relay,
     x_recv,
     s_send,
     s_recv,
@@ -64,9 +65,10 @@
     rows, width = out.shape
     chips = tps // 2
     chip, core = tp // 2, tp % 2
-    peers = [
-        ((chip + i) % chips) * 2 + (core + b) % 2 for i in range(1, chips) for b in range(2)
-    ] + [chip * 2 + (core + 1) % 2]
+    partner = chip * 2 + (core + 1) % 2
+    twins = [((chip + i) % chips) * 2 + core for i in range(1, chips)]
+    crosses = [((chip + i) % chips) * 2 + (core + 1) % 2 for i in range(1, chips)]
+    peers = twins + [partner]
     other_grps = [(g + d) % grps for d in range(1, grps)]
 
     barrier = pltpu.get_barrier_semaphore()
@@ -86,22 +88,23 @@
     inner = jnp.where(f > 0, 1, 0) + jnp.where(f < planes - 1, 1, 0)
     pl.semaphore_wait(barrier, len(peers) + len(other_grps) + inner)
 
-    def value_copy(phase, peer, slot):
+    def value_copy(phase, block, peer, relay=False):
         ref = input_all if phase == 0 else value_all.at[phase - 1]
+        fresh = phase == 0 and not relay
         return pltpu.make_async_remote_copy(
-            src_ref=payload if phase == 0 else ref.at[tp],
-            dst_ref=ref.at[slot],
-            send_sem=x_send.at[phase, peer],
-            recv_sem=x_recv.at[phase, slot],
+            src_ref=payload if fresh else ref.at[block],
+            dst_ref=ref.at[block],
+            send_sem=x_relay.at[phase, block] if relay else x_send.at[phase, peer],
+            recv_sem=x_recv.at[phase, block],
             device_id={"tp": peer},
             device_id_type=MESH,
         )
 
-    def sum_copy(phase, peer, slot):
+    def sum_copy(phase, block, slot, peer):
         return pltpu.make_async_remote_copy(
-            src_ref=parts.at[phase, peer],
+            src_ref=parts.at[phase, block],
             dst_ref=sums.at[phase, slot],
-            send_sem=s_send.at[phase, peer],
+            send_sem=s_send.at[phase, block],
             recv_sem=s_recv.at[phase, slot],
             device_id={"tp": peer},
             device_id_type=MESH,
@@ -161,8 +164,6 @@
         )
 
     def send_own(piece):
-        if piece >= len(pieces):
-            return
 
         @pl.when(f < planes - 1)
         def _():
@@ -173,7 +174,8 @@
             z_copy(piece, f, -1, own=True).start()
 
     def pass_on(piece):
-        send_own(piece + 2)
+        if piece + 1 < mixer_start:
+            send_own(piece + 1)
         for hop in range(1, planes):
 
             @pl.when(f >= hop)
@@ -200,6 +202,8 @@
 
     def of(*numbers):
         return [p for p, (number, part) in enumerate(pieces) if number in numbers]
+
+    mixer_start = of(3)[0]
 
     def arrive(*numbers):
         for number in numbers:
@@ -223,8 +227,11 @@
     row_tile = 32
 
     def scale_values(phase):
-        for peer in peers:
-            value_copy(phase, peer, peer).wait_recv()
+        for twin in twins:
+            value_copy(phase, twin, partner).wait_recv()
+            value_copy(phase, twin, partner, relay=True).start()
+        for block in [partner] + crosses:
+            value_copy(phase, block, partner).wait_recv()
         ref = input_all if phase == 0 else value_all.at[phase - 1]
 
         def body(step, carry):
@@ -260,30 +267,41 @@
     def project(phase, left, right_all):
         ratio = planes // tps
         block = right_all.shape[2]
-        for peer in peers + [tp]:
+
+        def compute(block_of):
             for piece in range(ratio):
-                parts[phase, peer, :, piece * block : (piece + 1) * block] = jnp.dot(
-                    left[...], right_all[peer * ratio + piece], preferred_element_type=F32
+                parts[phase, block_of, :, piece * block : (piece + 1) * block] = jnp.dot(
+                    left[...], right_all[block_of * ratio + piece], preferred_element_type=F32
                 ).astype(BF16)
-            if peer is not tp:
-                sum_copy(phase, peer, tp).start()
+
+        for twin, cross in zip(twins, crosses):
+            compute(cross)
+            sum_copy(phase, cross, twin, partner).start()
+        for twin, cross in zip(twins, crosses):
+            compute(twin)
+            sum_copy(phase, cross, cross, partner).wait_recv()
+            parts[phase, twin] = (
+                parts[phase, twin].astype(F32) + sums[phase, cross].astype(F32)
+            ).astype(BF16)
+            sum_copy(phase, twin, tp, twin).start()
+        compute(partner)
+        sum_copy(phase, partner, tp, partner).start()
+        compute(tp)
 
     def total_of(phase):
-        for peer in peers:
-            sum_copy(phase, peer, peer).wait_recv()
         total = parts[phase, tp].astype(F32)
-        for peer in peers:
+        for peer in [partner] + twins:
+            sum_copy(phase, peer, peer, partner).wait_recv()
             total = total + sums[phase, peer].astype(F32)
         return total
 
     def spread(phase):
         for peer in peers:
-            value_copy(phase, peer, tp).start()
+            value_copy(phase, tp, peer).start()
 
     local_input().start()
     spread(0)
     send_own(0)
-    send_own(1)
     for number in range(len(weights)):
         local_copy(number).start()
     first_pieces = of(0, 1)
@@ -298,6 +316,8 @@
     hidden_units()
     for piece in of(2)[1:]:
         pass_on(piece)
+    for piece in range(mixer_start, len(pieces)):
+        send_own(piece)
     arrive(2)
     project(0, hidden, down_all)
 
@@ -349,8 +369,11 @@
 
     for phase in range(3):
         for peer in peers:
-            value_copy(phase, peer, tp).wait_send()
-            sum_copy(phase, peer, tp).wait_send()
+            value_copy(phase, tp, peer).wait_send()
+        for twin in twins:
+            value_copy(phase, twin, partner, relay=True).wait_send()
+        for block in crosses + twins + [partner]:
+            sum_copy(phase, block, tp, partner).wait_send()
     for piece in range(len(pieces)):
 
         @pl.when(f < planes - 1)
@@ -407,7 +430,8 @@
     )
     units = ffn_gate_w.shape[1]
     channels = pool_in_w.shape[1]
-    wanted = (2, 2, 2, 1, 1, 1)
+    fine = max(16 // planes, 1)
+    wanted = (fine, fine, fine, max(fine // 4, 1), max(fine // 2, 1), max(fine // 4, 1))
     shards = (ffn_gate_w, ffn_up_w, ffn_down_w, pool_in_w, mixer_gate_w, mixer_out_w)
     piece_counts = tuple(
         ceil_pieces(shard.shape[0] // grps, count) for shard, count in zip(shards, wanted)
@@ -447,6 +471,7 @@
             dma((3, tps)),
             dma((3, tps)),
             dma((3, tps)),
+            dma((3, tps)),
         ],
         compiler_params=pltpu.CompilerParams(
             collective_id=0, has_side_effects=True, vmem_limit_bytes=60 * 1024 * 1024

time: 300 us -> 266 us (0.89)
  Pallas kernels: 294 us -> 262 us
    pallas_call x1, Pallas kernels: 294 us -> 262 us  [per_device(): pl.pallas_call(functools.partial(layer_kernel, (grps, planes, tps, piece_...]
where the time goes in v2:
time: 266 us
  Pallas kernels  262 us (98%)
    pallas_call x1, Pallas kernels, per_device(): pl.pallas_call(functools.partial(layer_kernel, (grps, planes, tps, piece_...  262 us

profile of v2, /device:TPU:0, one launch (start us, length us, event | category | flops | bytes accessed | tf_op | source)
XLA Modules:
  0.0 266.1 jit_solution(8543862485681216470)
XLA Ops:
  0.0 0.7 fusion.4
  0.7 1.8 pad_maximum_fusion.payload
  2.5 261.8 %shard_map.118 = bf16[384,512]{1,0:T(8,128)(2,1)} custom-call(bf16[400,512]{1,0:T(8,128)(2,1)} %pad_maximum_fusion.payload, bf16[512,1536]{1,0:T(8,128)(2,1)} %gate_w.1, bf16[512,1536]{1,0:T(8,128)(2,1)} %up_w.1, bf16[1536,512]{1,0:T(8,128)(2,1)} %down_w.1, bf16[512,256]{1,0:T(8,128)(2,1)} %pool_w.1, bf16[512,512]{1,0:T(8,128)(2,1)} %mgate_w.1, ...), custom_call_target="tpu_custom_call" | custom-call | tf_op jit(solution)/shard_map/pallas_call | solution.py:443
  264.3 1.8 copy.14
